TPU v7x, 32 devices: a whole 2x2x4 slice. The times are simulated.
32 devices in a mesh: kv: 16 (over z, y, x), tp: 2 (over core).
Axes of the slice: x: 2, y: 2, z: 4, core: 2. Of those that a mesh axis runs over, the one named last changes fastest.
Arguments:
- tokens: bfloat16 [8, 2048, 2048], P(None, 'kv'), may hold values from -32 to 32, as said below
- w_query: bfloat16 [2048, 1024], P(None, 'tp'), may hold values from -0.125 to 0.125
- w_key: bfloat16 [2048, 512], P(None, 'tp'), may hold values from -0.125 to 0.125
- w_value: bfloat16 [2048, 512], P(None, 'tp'), may hold values from -0.125 to 0.125
- w_output: bfloat16 [1024, 2048], P(None, 'tp'), may hold values from -3 to 3
- chosen: int32 [8, 16, 32], P(None, 'kv'), may hold values from -1 to 15, as said below
- lengths: int32 [8], replicated, may hold values from 1 to 2048, 5632 in all
Outputs:
- mixed: bfloat16 [8, 2048, 2048], P(None, 'kv', 'tp')
Inputs may be any that keep to these rules, and one draw needn't show every extreme that they name: chosen[s, b] lists distinct blocks of sequence s, none above b; its first entry is b; entries after the named ones are -1. For b >= 1 and each c < b, at most 4 of the 8 lists chosen[:, b] name block c, and exactly 4 of them name block b - 1. lengths[s] is the number of live positions of sequence s; the largest is 2048. `tokens`: activations of order one; some rows may be much larger.
All inputs are finite; a program needn't handle non-finite values.
Results may differ from a plain program's by a relative error of at most 0.012.
The roundings to bfloat16 on the way count: a program that leaves them out, or rounds other values in their place, can miss the bound.
Values may be sent and summed in bfloat16 or wider, within the bound.
A program may use at most 128 MiB of HBM per device.

v0:
```python
import jax
import jax.numpy as jnp
from jax import lax
from jax.sharding import PartitionSpec as P

HEADS = 16
KV_HEADS = 8
HEAD_DIM = 64
CAP = 4


def per_device(tokens, w_query, w_key, w_value, w_output, chosen, lengths):
    seq_count, block_len, model_width = tokens.shape
    flat_rows = tokens.reshape(seq_count * block_len, model_width)
    queries = jnp.dot(flat_rows, w_query, preferred_element_type=jnp.float32).astype(jnp.bfloat16)
    key_proj = jnp.dot(flat_rows, w_key, preferred_element_type=jnp.float32).astype(jnp.bfloat16)
    value_proj = jnp.dot(flat_rows, w_value, preferred_element_type=jnp.float32).astype(
        jnp.bfloat16
    )
    key_width = key_proj.shape[1]
    local_blocks = jnp.concatenate([key_proj, value_proj], axis=1).reshape(
        seq_count, block_len, 2 * key_width
    )
    shard_member = lax.axis_index("kv")
    kv_devices = lax.axis_size("kv")
    picked = chosen[:, 0, :]
    clipped = jnp.maximum(picked, 0)
    seq_index = jnp.arange(seq_count, dtype=jnp.int32)
    owners = jnp.arange(kv_devices, dtype=jnp.int32)
    wanted = (
        jnp.any(picked[:, :, None] == owners[None, None, :], axis=1)
        & (owners != shard_member)[None, :]
    )
    wanted = wanted.T
    ranked = jnp.cumsum(wanted.astype(jnp.int32), axis=1) - 1
    slot_hit = wanted[:, :, None] & (
        ranked[:, :, None] == jnp.arange(CAP, dtype=jnp.int32)[None, None, :]
    )
    request = jnp.sum(slot_hit.astype(jnp.int32) * (seq_index + 1)[None, :, None], axis=1) - 1
    incoming = lax.all_to_all(request, "kv", split_axis=0, concat_axis=0, tiled=True)
    outgoing = local_blocks[jnp.maximum(incoming, 0)]
    arrived = lax.all_to_all(outgoing, "kv", split_axis=0, concat_axis=0, tiled=True)
    key_lookup = jnp.concatenate(
        [local_blocks, arrived.reshape(kv_devices * CAP, block_len, 2 * key_width)], axis=0
    )
    rank_at = jnp.take_along_axis(ranked.T, clipped, axis=1)
    source = jnp.where(
        picked == shard_member, seq_index[:, None], seq_count + clipped * CAP + rank_at
    )
    group_size = HEADS // KV_HEADS
    local_kv_heads = key_width // HEAD_DIM
    query_pos = shard_member * block_len + jnp.arange(block_len, dtype=jnp.int32)
    score_scale = HEAD_DIM ** (-0.5)

    def attend(packed):
        query_rows, source_row, pick_row, length = packed
        fetched = key_lookup[source_row]
        slot_count = pick_row.shape[0]
        key_rows = fetched[:, :, :key_width].reshape(
            slot_count * block_len, local_kv_heads, HEAD_DIM
        )
        value_rows = fetched[:, :, key_width:].reshape(
            slot_count * block_len, local_kv_heads, HEAD_DIM
        )
        grouped = query_rows.reshape(block_len, local_kv_heads, group_size, HEAD_DIM)
        scores = (
            jnp.einsum("qkgd,nkd->kgqn", grouped, key_rows, preferred_element_type=jnp.float32)
            * score_scale
        )
        key_pos = (
            pick_row[:, None] * block_len + jnp.arange(block_len, dtype=jnp.int32)[None, :]
        ).reshape(-1)
        listed = jnp.repeat(pick_row >= 0, block_len)
        allowed = (
            listed[None, :] & (key_pos[None, :] <= query_pos[:, None]) & (key_pos[None, :] < length)
        )
        masked = jnp.where(allowed, scores, -1e30)
        row_max = jnp.max(masked, axis=-1, keepdims=True)
        exponent = jnp.exp(masked - row_max)
        weights = (exponent / jnp.sum(exponent, axis=-1, keepdims=True)).astype(jnp.bfloat16)
        mixed_heads = jnp.einsum(
            "kgqn,nkd->qkgd", weights, value_rows, preferred_element_type=jnp.float32
        )
        live_rows = (query_pos < length)[:, None, None, None]
        return jnp.where(live_rows, mixed_heads, 0.0).astype(jnp.bfloat16).reshape(block_len, -1)

    attended = lax.map(attend, (queries.reshape(seq_count, block_len, -1), source, picked, lengths))
    attended_rows = attended.reshape(seq_count * block_len, -1)
    summed = jnp.dot(
        lax.all_gather(attended_rows, "tp", axis=1, tiled=True),
        w_output,
        preferred_element_type=jnp.float32,
    )
    return summed.astype(jnp.bfloat16).reshape(seq_count, block_len, -1)


def solution(mesh):
    return jax.shard_map(
        per_device,
        mesh=mesh,
        in_specs=(
            P(None, "kv", None),
            P(None, "tp"),
            P(None, "tp"),
            P(None, "tp"),
            P(None, "tp"),
            P(None, "kv", None),
            P(),
        ),
        out_specs=P(None, "kv", "tp"),
        check_vma=False,
    )
```

profile of v0, /device:TPU:0, one launch (start us, length us, event | category | flops | bytes accessed | tf_op | source)
XLA Modules:
  0.0 852.4 jit_solution(16968193628493152081)
XLA Ops:
  8.4 8.3 all-to-all-start
  24.8 5.5 gather_fusion.1
  30.3 6.8 all-to-all-start.1
  38.8 6.2 convolution_convert_fusion.1
  45.0 147.7 %all-to-all-done.1 = bf16[16,4,128,512]{3,2,1,0:T(8,128)(2,1)} async-done(((bf16[16,4,128,512]{3,2,1,0:T(8,128)(2,1)}), bf16[16,4,128,512]{3,2,1,0:T(8,128)(2,1)}, u32[]{:S(2)}, u32[]{:S(2)}) %all-to-all-start.1) | async-done | bytes 8388640 | tf_op jit(solution)/shard_map/all_to_all | solution.py:42
  192.7 7.8 pad_maximum_fusion
  200.5 595.3 %while.11 = (s32[]{:T(128)}, bf16[8,128,512]{2,1,0:T(8,128)(2,1)}, s32[8]{0:T(128)S(1)}, s32[8,32]{1,0:T(8,128)S(1)}, bf16[72,128,512]{2,1,0:T(8,128)(2,1)}, /*i...) while((s32[]{:T(128)}, bf16[8,128,512]{2,1,0:T(8,128)(2,1)}, ...), condition=%wide.region_6.7_spmd.clone, body=%wide.region_3.0_spmd.clone.sunk | while | flops 1109018112 | bytes 107281480 | solution.py:87
  205.4 6.4 gather_fusion
  211.8 4.7 fusion.48
  226.3 9.7 %fusion.49 = f32[4,4096,128,2]{2,1,3,0:T(8,128)} fusion(bf16[128,4,2,64]{0,3,2,1:T(8,128)(2,1)S(1)} %bitcast.106, bf16[4096,4,64,1]{0,2,1,3:T(8,128)(2,1)} %reshape.219), kind=kOutput, calls=%fused_computation.13.clone.1 | convolution fusion | flops 536870912 | bytes 19005440 | tf_op jit(solution)/shard_map/while/body/eval_jaxpr/qkgd,nkd->kgqn/dot_general | solution.py:67
  236.0 20.9 %fusion.50 = (f32[4,2,128]{2,1,0:T(2,128)S(1)}, f32[4,2,128,4096]{2,3,1,0:T(8,128)}) fusion(f32[4,4096,128,2]{2,1,3,0:T(8,128)} %fusion.49, pred[128,4096]{0,1:T(8,128)(4,1)S(1)} %and_and_fusion.2), kind=kOutput, calls=%fused_computation.60.clone.1 | output fusion | flops 25169920 | bytes 34082816 | tf_op jit(solution)/shard_map/while/body/eval_jaxpr/sub | solution.py:79
  266.2 8.0 fusion.51
  279.8 6.4 gather_fusion
  286.2 4.7 fusion.48
  300.7 9.7 %fusion.49 = f32[4,4096,128,2]{2,1,3,0:T(8,128)} fusion(bf16[128,4,2,64]{0,3,2,1:T(8,128)(2,1)S(1)} %bitcast.106, bf16[4096,4,64,1]{0,2,1,3:T(8,128)(2,1)} %reshape.219), kind=kOutput, calls=%fused_computation.13.clone.1 | convolution fusion | flops 536870912 | bytes 19005440 | tf_op jit(solution)/shard_map/while/body/eval_jaxpr/qkgd,nkd->kgqn/dot_general | solution.py:67
  310.4 20.9 %fusion.50 = (f32[4,2,128]{2,1,0:T(2,128)S(1)}, f32[4,2,128,4096]{2,3,1,0:T(8,128)}) fusion(f32[4,4096,128,2]{2,1,3,0:T(8,128)} %fusion.49, pred[128,4096]{0,1:T(8,128)(4,1)S(1)} %and_and_fusion.2), kind=kOutput, calls=%fused_computation.60.clone.1 | output fusion | flops 25169920 | bytes 34082816 | tf_op jit(solution)/shard_map/while/body/eval_jaxpr/sub | solution.py:79
  340.6 8.0 fusion.51
  354.2 6.4 gather_fusion
  360.6 4.7 fusion.48
  375.1 9.7 %fusion.49 = f32[4,4096,128,2]{2,1,3,0:T(8,128)} fusion(bf16[128,4,2,64]{0,3,2,1:T(8,128)(2,1)S(1)} %bitcast.106, bf16[4096,4,64,1]{0,2,1,3:T(8,128)(2,1)} %reshape.219), kind=kOutput, calls=%fused_computation.13.clone.1 | convolution fusion | flops 536870912 | bytes 19005440 | tf_op jit(solution)/shard_map/while/body/eval_jaxpr/qkgd,nkd->kgqn/dot_general | solution.py:67
  384.8 20.9 %fusion.50 = (f32[4,2,128]{2,1,0:T(2,128)S(1)}, f32[4,2,128,4096]{2,3,1,0:T(8,128)}) fusion(f32[4,4096,128,2]{2,1,3,0:T(8,128)} %fusion.49, pred[128,4096]{0,1:T(8,128)(4,1)S(1)} %and_and_fusion.2), kind=kOutput, calls=%fused_computation.60.clone.1 | output fusion | flops 25169920 | bytes 34082816 | tf_op jit(solution)/shard_map/while/body/eval_jaxpr/sub | solution.py:79
  415.0 8.0 fusion.51
  428.6 6.4 gather_fusion
  435.0 4.7 fusion.48
  449.5 9.7 %fusion.49 = f32[4,4096,128,2]{2,1,3,0:T(8,128)} fusion(bf16[128,4,2,64]{0,3,2,1:T(8,128)(2,1)S(1)} %bitcast.106, bf16[4096,4,64,1]{0,2,1,3:T(8,128)(2,1)} %reshape.219), kind=kOutput, calls=%fused_computation.13.clone.1 | convolution fusion | flops 536870912 | bytes 19005440 | tf_op jit(solution)/shard_map/while/body/eval_jaxpr/qkgd,nkd->kgqn/dot_general | solution.py:67
  459.2 20.9 %fusion.50 = (f32[4,2,128]{2,1,0:T(2,128)S(1)}, f32[4,2,128,4096]{2,3,1,0:T(8,128)}) fusion(f32[4,4096,128,2]{2,1,3,0:T(8,128)} %fusion.49, pred[128,4096]{0,1:T(8,128)(4,1)S(1)} %and_and_fusion.2), kind=kOutput, calls=%fused_computation.60.clone.1 | output fusion | flops 25169920 | bytes 34082816 | tf_op jit(solution)/shard_map/while/body/eval_jaxpr/sub | solution.py:79
  489.4 8.0 fusion.51
  503.0 6.4 gather_fusion
  509.4 4.7 fusion.48
  523.9 9.7 %fusion.49 = f32[4,4096,128,2]{2,1,3,0:T(8,128)} fusion(bf16[128,4,2,64]{0,3,2,1:T(8,128)(2,1)S(1)} %bitcast.106, bf16[4096,4,64,1]{0,2,1,3:T(8,128)(2,1)} %reshape.219), kind=kOutput, calls=%fused_computation.13.clone.1 | convolution fusion | flops 536870912 | bytes 19005440 | tf_op jit(solution)/shard_map/while/body/eval_jaxpr/qkgd,nkd->kgqn/dot_general | solution.py:67
  533.6 20.9 %fusion.50 = (f32[4,2,128]{2,1,0:T(2,128)S(1)}, f32[4,2,128,4096]{2,3,1,0:T(8,128)}) fusion(f32[4,4096,128,2]{2,1,3,0:T(8,128)} %fusion.49, pred[128,4096]{0,1:T(8,128)(4,1)S(1)} %and_and_fusion.2), kind=kOutput, calls=%fused_computation.60.clone.1 | output fusion | flops 25169920 | bytes 34082816 | tf_op jit(solution)/shard_map/while/body/eval_jaxpr/sub | solution.py:79
  563.8 8.0 fusion.51
  577.4 6.4 gather_fusion
  583.8 4.7 fusion.48
  598.3 9.7 %fusion.49 = f32[4,4096,128,2]{2,1,3,0:T(8,128)} fusion(bf16[128,4,2,64]{0,3,2,1:T(8,128)(2,1)S(1)} %bitcast.106, bf16[4096,4,64,1]{0,2,1,3:T(8,128)(2,1)} %reshape.219), kind=kOutput, calls=%fused_computation.13.clone.1 | convolution fusion | flops 536870912 | bytes 19005440 | tf_op jit(solution)/shard_map/while/body/eval_jaxpr/qkgd,nkd->kgqn/dot_general | solution.py:67
  608.0 20.9 %fusion.50 = (f32[4,2,128]{2,1,0:T(2,128)S(1)}, f32[4,2,128,4096]{2,3,1,0:T(8,128)}) fusion(f32[4,4096,128,2]{2,1,3,0:T(8,128)} %fusion.49, pred[128,4096]{0,1:T(8,128)(4,1)S(1)} %and_and_fusion.2), kind=kOutput, calls=%fused_computation.60.clone.1 | output fusion | flops 25169920 | bytes 34082816 | tf_op jit(solution)/shard_map/while/body/eval_jaxpr/sub | solution.py:79
  638.2 8.0 fusion.51
  651.8 6.4 gather_fusion
  672.7 9.7 %fusion.49 = f32[4,4096,128,2]{2,1,3,0:T(8,128)} fusion(bf16[128,4,2,64]{0,3,2,1:T(8,128)(2,1)S(1)} %bitcast.106, bf16[4096,4,64,1]{0,2,1,3:T(8,128)(2,1)} %reshape.219), kind=kOutput, calls=%fused_computation.13.clone.1 | convolution fusion | flops 536870912 | bytes 19005440 | tf_op jit(solution)/shard_map/while/body/eval_jaxpr/qkgd,nkd->kgqn/dot_general | solution.py:67
  682.4 20.9 %fusion.50 = (f32[4,2,128]{2,1,0:T(2,128)S(1)}, f32[4,2,128,4096]{2,3,1,0:T(8,128)}) fusion(f32[4,4096,128,2]{2,1,3,0:T(8,128)} %fusion.49, pred[128,4096]{0,1:T(8,128)(4,1)S(1)} %and_and_fusion.2), kind=kOutput, calls=%fused_computation.60.clone.1 | output fusion | flops 25169920 | bytes 34082816 | tf_op jit(solution)/shard_map/while/body/eval_jaxpr/sub | solution.py:79
  712.6 8.0 fusion.51
  726.2 6.4 gather_fusion
  732.6 4.7 fusion.48
  747.1 9.7 %fusion.49 = f32[4,4096,128,2]{2,1,3,0:T(8,128)} fusion(bf16[128,4,2,64]{0,3,2,1:T(8,128)(2,1)S(1)} %bitcast.106, bf16[4096,4,64,1]{0,2,1,3:T(8,128)(2,1)} %reshape.219), kind=kOutput, calls=%fused_computation.13.clone.1 | convolution fusion | flops 536870912 | bytes 19005440 | tf_op jit(solution)/shard_map/while/body/eval_jaxpr/qkgd,nkd->kgqn/dot_general | solution.py:67
  756.8 20.9 %fusion.50 = (f32[4,2,128]{2,1,0:T(2,128)S(1)}, f32[4,2,128,4096]{2,3,1,0:T(8,128)}) fusion(f32[4,4096,128,2]{2,1,3,0:T(8,128)} %fusion.49, pred[128,4096]{0,1:T(8,128)(4,1)S(1)} %and_and_fusion.2), kind=kOutput, calls=%fused_computation.60.clone.1 | output fusion | flops 25169920 | bytes 34082816 | tf_op jit(solution)/shard_map/while/body/eval_jaxpr/sub | solution.py:79
  787.0 8.0 fusion.51
  795.8 44.5 %all-gather.2.cloned.1.call-done = bf16[1024,1024]{1,0:T(8,128)(2,1)} async-done(((bf16[1024,512]{1,0:T(8,128)(2,1)}), bf16[1024,1024]{1,0:T(8,128)(2,1)}) %all-gather.2.cloned.1.call-update) | async-done | bytes 2097168 | tf_op jit(solution)/shard_map/all_gather | solution.py:90
  840.3 5.2 convolution_convert_fusion
  (189 shorter events, 213.4 us)
Async XLA Ops:
  6.5 833.8 %copy-start = (bf16[1024,1024]{1,0:T(8,128)(2,1)S(1)}, bf16[1024,1024]{1,0:T(8,128)(2,1)}, u32[]{:S(2)}) copy-start(bf16[1024,1024]{1,0:T(8,128)(2,1)} %param.13) | copy-start | bytes 6291460
  8.4 16.3 %all-to-all-start = ((s32[16,1,4]{2,1,0:T(1,128)}), s32[16,1,4]{2,1,0:T(1,128)S(1)}, u32[]{:S(2)}, u32[]{:S(2)}) async-start(s32[16,1,4]{2,1,0:T(1,128)} %copy.40), calls=%async_computation | async-start | bytes 16384 | tf_op jit(solution)/shard_map/all_to_all | solution.py:40
  16.8 4.0 copy-start.2
  16.8 4.0 copy-start.3
  30.3 6.9 copy-start.1
  30.3 162.5 %all-to-all-start.1 = ((bf16[16,4,128,512]{3,2,1,0:T(8,128)(2,1)}), bf16[16,4,128,512]{3,2,1,0:T(8,128)(2,1)}, u32[]{:S(2)}, u32[]{:S(2)}) async-start(bf16[16,4,128,512]{3,2,1,0:T(8,128)(2,1)} %bitcast.105), calls=%async_computation.1 | async-start | bytes 16777216 | tf_op jit(solution)/shard_map/all_to_all | solution.py:42
  37.1 803.2 %all-gather.2.cloned.1.call-start = ((), (), s32[]{:S(2)}) async-start(), calls=%async_computation.2 | async-start | bytes 3145728 | tf_op jit(solution)/shard_map/all_gather | solution.py:90
  192.7 7.8 copy-start.4
Sparse Core Ops, SparseCore 0:
  795.9 44.3 all-gather.1
where the time goes:
time: 856 us; the launch traced here: 852 us
  local copies, waits for them, and re-layouts  258 us (30%)
  other arithmetic  215 us (25%)
  waiting for transfers between devices  192 us (22%)
  matrix products  158 us (18%)
  starting transfers between devices  15.2 us (2%)
  between operations  13.5 us (2%)
    sub x8, other arithmetic, attend(): exponent = jnp.exp(masked - row_max)  167 us
    all_to_all x1, waiting for transfers between devices, per_device(): lax.all_to_all(outgoing, 'kv', split_axis=0, concat_axis=0, tiled=True)  148 us
    dot_general x8, matrix products, attend(): jnp.einsum('qkgd,nkd->kgqn', grouped, key_rows, preferred_element_type=jn...  77.5 us
    slice x16, local copies, waits for them, and re-layouts, attend(): fetched[:, :, key_width:]  74.6 us
    dot_general x8, matrix products, attend(): jnp.einsum('kgqn,nkd->qkgd', weights, value_rows, preferred_element_type=...  63.9 us
    gather x8, local copies, waits for them, and re-layouts, attend(): fetched = key_lookup[source_row]  51.4 us
    all_gather x1, waiting for transfers between devices, per_device(): lax.all_gather(attended_rows, 'tp', axis=1, tiled=True)  44.5 us
    slice x8, local copies, waits for them, and re-layouts, attend(): fetched[:, :, :key_width]  36.4 us
  transfers between devices with their start and end apart: 3, of which 2 were waited for; matrix products, arithmetic and copies ran while one was open for 2% of the time, Pallas kernels for 0%

commit v1 on v0

v1 whole, which is shorter than its diff:
```python
import functools

import jax
import jax.numpy as jnp
from jax import lax
from jax.experimental import pallas as pl
from jax.experimental.pallas import tpu as pltpu
from jax.sharding import PartitionSpec as P

HEADS = 16
KV_HEADS = 8
HEAD_DIM = 64
CAP = 4
LANES = 128
MESH = pl.DeviceIdType.MESH
VMEM_LIMIT = 60 * 1024 * 1024


def blocks_to(dest, n, block_len, cap):
    seq_len = n * block_len
    spare = seq_len * 7 // 4
    count = jnp.int32(1)
    for k in range(1, cap):
        count = count + (k * (dest * block_len + 1) <= spare).astype(jnp.int32)
    return count


def greet(axis, me, n):
    barrier = pltpu.get_barrier_semaphore()
    for k in range(1, n):
        pl.semaphore_signal(
            barrier, inc=1, device_id={axis: lax.rem(me + k, n)}, device_id_type=MESH
        )
    return barrier


def project_kernel(
    n, steps, x_ref, wq_ref, wk_ref, wv_ref, chosen_ref, len_ref,
    q_ref, kv_ref, rank_ref, got_ref, incoming_ref, req_ref, send_sem, recv_sem,
):
    step = pl.program_id(0)
    me = lax.axis_index("kv")
    seqs, slots = chosen_ref.shape
    seqs_now, block_len, width = x_ref.shape
    kw = wk_ref.shape[1]

    def request_copy(dest, slot, k=0):
        return pltpu.make_async_remote_copy(
            src_ref=req_ref,
            dst_ref=incoming_ref.at[slot],
            send_sem=send_sem.at[k],
            recv_sem=recv_sem.at[slot],
            device_id={"kv": dest},
            device_id_type=MESH,
        )

    @pl.when(step == 0)
    def _():
        greet("kv", me, n)
        owner = lax.broadcasted_iota(jnp.int32, (seqs, LANES), 1)
        picked = chosen_ref[...]
        wanted = jnp.zeros((seqs, LANES), jnp.int32)
        for j in range(slots):
            wanted = wanted | (picked[:, j : j + 1] == owner).astype(jnp.int32)
        live = len_ref[...] > me * block_len
        wanted = jnp.where(live & (owner < me), wanted, 0)
        count = jnp.zeros((1, LANES), jnp.int32)
        rows = [jnp.zeros((1, LANES), jnp.int32) for _ in range(CAP)]
        ranks = []
        for s in range(seqs):
            hit = wanted[s : s + 1]
            ranks.append(count)
            for r in range(CAP):
                rows[r] = jnp.where((hit > 0) & (count == r), s, rows[r])
            count = count + hit
        rank_ref[...] = jnp.concatenate(ranks, axis=0)
        fill = [jnp.zeros((8 - CAP, LANES), jnp.int32)]
        req_ref[...] = jnp.concatenate(rows + fill, axis=0)
        incoming_ref[me] = jnp.zeros((8, LANES), jnp.int32)

    rows = x_ref[...].reshape(seqs_now * block_len, width)
    scale = HEAD_DIM ** (-0.5)

    def project(w_ref):
        out = jnp.dot(rows, w_ref[...], preferred_element_type=jnp.float32).astype(jnp.bfloat16)
        return out.reshape(seqs_now, block_len, -1)

    q_ref[...] = project(wq_ref) * jnp.bfloat16(scale)
    kv_ref[:, :, :kw] = project(wk_ref)
    kv_ref[:, :, kw:] = project(wv_ref)

    @pl.when(step == 0)
    def _():
        pl.semaphore_wait(pltpu.get_barrier_semaphore(), n - 1)
        for k in range(1, n):
            request_copy(lax.rem(me + k, n), me, k).start()

    @pl.when(step == steps - 1)
    def _():
        for k in range(1, n):
            request_copy(lax.rem(me + k, n), me, k).wait_send()
        for k in range(1, n):
            other = lax.rem(me + k, n)
            request_copy(other, other).wait_recv()
        got_ref[...] = incoming_ref[...]


def exchange_kernel(n, idx_ref, kv_ref, arrived_ref, pack_ref, send_sem, recv_sem):
    me = lax.axis_index("kv")
    block_len = kv_ref.shape[1]
    barrier = greet("kv", me, n)

    def copy(k, dest, slot, blocks):
        return pltpu.make_async_remote_copy(
            src_ref=pack_ref.at[k, pl.ds(0, blocks)],
            dst_ref=arrived_ref.at[slot, pl.ds(0, blocks)],
            send_sem=send_sem.at[k],
            recv_sem=recv_sem.at[slot],
            device_id={"kv": dest},
            device_id_type=MESH,
        )

    def each_send(k, act):
        dest = me + k
        count = blocks_to(dest, n, block_len, CAP)
        for blocks in range(1, CAP + 1):
            @pl.when((dest < n) & (count == blocks))
            def _():
                act(copy(k, dest, me, blocks))

    for k in range(1, n + 1):
        if k < n:
            @pl.when(me + k < n)
            def _():
                for r in range(CAP):
                    pack_ref[k, r] = kv_ref[idx_ref[(me + k) * CAP + r]]
        if k == 2:
            pl.semaphore_wait(barrier, n - 1)
        if k >= 2:
            each_send(k - 1, lambda c: c.start())
    for k in range(1, n):
        each_send(k, lambda c: c.wait_send())
    mine = blocks_to(me, n, block_len, CAP)
    for k in range(1, n):
        for blocks in range(1, CAP + 1):
            @pl.when((me - k >= 0) & (mine == blocks))
            def _():
                copy(k, me - k, me - k, blocks).wait_recv()


def attend_kernel(
    len_ref, pick_ref, rank_ref, q_ref, kv_ref, arr_ref, out_ref,
    qs_ref, s_ref, m_ref, l_ref, acc_ref,
):
    s = pl.program_id(0)
    me = lax.axis_index("kv")
    block_len, qw = q_ref.shape[1:]
    kw = kv_ref.shape[2] // 2
    w = min(LANES, kw)
    tiles, per_tile = kw // w, w // HEAD_DIM
    group = HEADS // KV_HEADS
    heads = group * per_tile
    rows = heads * block_len
    slots = pick_ref.shape[1]
    length = len_ref[s]
    live = length > me * block_len

    @pl.when(jnp.logical_not(live))
    def _():
        out_ref[...] = jnp.zeros(out_ref.shape, out_ref.dtype)

    @pl.when(live)
    def _():
        count = jnp.int32(0)
        for j in range(slots):
            count = count + (pick_ref[s, j] >= 0).astype(jnp.int32)
        zero = jnp.zeros((block_len, HEAD_DIM), jnp.bfloat16)
        for t in range(tiles):
            for i in range(heads):
                h = t * heads + i
                own = q_ref[0, :, h * HEAD_DIM : (h + 1) * HEAD_DIM]
                parts = [own if i // group == p else zero for p in range(per_tile)]
                qs_ref[t, i * block_len : (i + 1) * block_len, :] = jnp.concatenate(parts, axis=1)

        def score(t, keys):
            return lax.dot_general(
                qs_ref[t], keys, (((1,), (1,)), ((), ())), preferred_element_type=jnp.float32
            )

        key_at = lax.broadcasted_iota(jnp.int32, (heads, block_len, block_len), 2)
        row_at = lax.broadcasted_iota(jnp.int32, (heads, block_len, block_len), 1)
        causal = (key_at <= row_at).reshape(rows, block_len)
        for t in range(tiles):
            first = jnp.where(causal, score(t, kv_ref[0, :, t * w : (t + 1) * w]), -1e30)
            s_ref[0, t] = first
            m_ref[t] = first

        def score_slot(j, carry):
            c = pick_ref[s, j]
            r = rank_ref[s, c]
            for t in range(tiles):
                got = score(t, arr_ref[c, r, :, t * w : (t + 1) * w])
                s_ref[j, t] = got
                m_ref[t] = jnp.maximum(m_ref[t], got)
            return carry

        lax.fori_loop(1, count, score_slot, 0)
        for t in range(tiles):
            top = jnp.max(m_ref[t], axis=1, keepdims=True)
            m_ref[t] = jnp.broadcast_to(top, (rows, block_len))
            p = jnp.exp(s_ref[0, t] - top)
            l_ref[t] = p
            acc_ref[t] = jnp.dot(
                p.astype(jnp.bfloat16),
                kv_ref[0, :, kw + t * w : kw + (t + 1) * w],
                preferred_element_type=jnp.float32,
            )

        def value_slot(j, carry):
            c = pick_ref[s, j]
            r = rank_ref[s, c]
            for t in range(tiles):
                p = jnp.exp(s_ref[j, t] - m_ref[t])
                l_ref[t] = l_ref[t] + p
                acc_ref[t] = acc_ref[t] + jnp.dot(
                    p.astype(jnp.bfloat16),
                    arr_ref[c, r, :, kw + t * w : kw + (t + 1) * w],
                    preferred_element_type=jnp.float32,
                )
            return carry

        lax.fori_loop(1, count, value_slot, 0)
        at = me * block_len + lax.broadcasted_iota(jnp.int32, (block_len, w), 0)
        for t in range(tiles):
            total = jnp.sum(l_ref[t], axis=1, keepdims=True)
            done = acc_ref[t] / total
            for i in range(heads):
                h = t * heads + i
                part = done[i * block_len : (i + 1) * block_len]
                part = jnp.where(at < length, part, 0.0).astype(jnp.bfloat16)
                lane = (i // group) * HEAD_DIM
                out_ref[0, :, h * HEAD_DIM : (h + 1) * HEAD_DIM] = part[:, lane : lane + HEAD_DIM]


def mix_kernel(tp, att_ref, w_ref, out_ref, held_ref, acc_ref, send_sem, recv_sem):
    me = lax.axis_index("tp")
    seqs, block_len, hw = att_ref.shape
    chunk = 2
    barrier = greet("tp", me, tp)
    pl.semaphore_wait(barrier, tp - 1)

    def copy(k, dest):
        return pltpu.make_async_remote_copy(
            src_ref=att_ref,
            dst_ref=held_ref.at[k - 1],
            send_sem=send_sem.at[k - 1],
            recv_sem=recv_sem.at[k - 1],
            device_id={"tp": dest},
            device_id_type=MESH,
        )

    for k in range(1, tp):
        copy(k, lax.rem(me + k, tp)).start()

    def term(rows, owner):
        weights = w_ref[pl.ds(pl.multiple_of(owner * hw, hw), hw), :]
        return jnp.dot(
            rows.reshape(chunk * block_len, hw), weights, preferred_element_type=jnp.float32
        ).reshape(chunk, block_len, -1)

    @pl.loop(0, seqs // chunk)
    def _(i):
        now = pl.ds(i * chunk, chunk)
        acc_ref[now] = term(att_ref[now], me)

    for k in range(1, tp):
        copy(k, lax.rem(me + k, tp)).wait()
        owner = lax.rem(me + tp - k, tp)

        @pl.loop(0, seqs // chunk)
        def _(i):
            now = pl.ds(i * chunk, chunk)
            total = acc_ref[now] + term(held_ref[k - 1, now], owner)
            if k < tp - 1:
                acc_ref[now] = total
            else:
                out_ref[now] = total.astype(out_ref.dtype)


def per_device(n, tp, tokens, w_query, w_key, w_value, w_output, chosen, lengths):
    seqs, block_len, width = tokens.shape
    qw, kw = w_query.shape[1], w_key.shape[1]
    bf16 = jnp.bfloat16
    picked = chosen[:, 0, :]
    vmem = pl.BlockSpec(memory_space=pltpu.VMEM)
    steps = 4
    part = seqs // steps

    def whole(shape):
        return pl.BlockSpec(shape, lambda i: (0,) * len(shape))

    def piece(last):
        return pl.BlockSpec((part, block_len, last), lambda i: (i, 0, 0))

    queries, local, rank, incoming = pl.pallas_call(
        functools.partial(project_kernel, n, steps),
        grid=(steps,),
        out_shape=(
            jax.ShapeDtypeStruct((seqs, block_len, qw), bf16),
            jax.ShapeDtypeStruct((seqs, block_len, 2 * kw), bf16),
            jax.ShapeDtypeStruct((seqs, LANES), jnp.int32),
            jax.ShapeDtypeStruct((n, 8, LANES), jnp.int32),
        ),
        in_specs=[
            piece(width), whole((width, qw)), whole((width, kw)), whole((width, kw)),
            whole(picked.shape), whole((seqs, 1)),
        ],
        out_specs=[piece(qw), piece(2 * kw), whole((seqs, LANES)), whole((n, 8, LANES))],
        scratch_shapes=[
            pltpu.VMEM((n, 8, LANES), jnp.int32),
            pltpu.VMEM((8, LANES), jnp.int32),
            pltpu.SemaphoreType.DMA((n,)),
            pltpu.SemaphoreType.DMA((n,)),
        ],
        compiler_params=pltpu.CompilerParams(
            collective_id=0, has_side_effects=True, vmem_limit_bytes=VMEM_LIMIT
        ),
    )(tokens, w_query, w_key, w_value, picked, lengths[:, None])

    shard = lax.axis_index("kv")
    asked = lax.dynamic_slice_in_dim(incoming[:, :CAP, :], shard, 1, axis=2)
    asked = jnp.clip(asked, 0, seqs - 1).reshape(n * CAP)

    arrived = pl.pallas_call(
        functools.partial(exchange_kernel, n),
        out_shape=jax.ShapeDtypeStruct((n, CAP, block_len, 2 * kw), bf16),
        in_specs=[pl.BlockSpec(memory_space=pltpu.SMEM), vmem],
        out_specs=pl.BlockSpec(memory_space=pl.ANY),
        scratch_shapes=[
            pltpu.VMEM((n, CAP, block_len, 2 * kw), bf16),
            pltpu.SemaphoreType.DMA((n,)),
            pltpu.SemaphoreType.DMA((n,)),
        ],
        compiler_params=pltpu.CompilerParams(
            collective_id=1, has_side_effects=True, vmem_limit_bytes=VMEM_LIMIT
        ),
    )(asked, local)

    w = min(LANES, kw)
    tiles = kw // w
    rows = (w // HEAD_DIM) * (HEADS // KV_HEADS) * block_len
    keep = min(picked.shape[1], n)

    def seq_spec(last):
        return pl.BlockSpec((1, block_len, last), lambda i, *_: (i, 0, 0))

    attended = pl.pallas_call(
        attend_kernel,
        out_shape=jax.ShapeDtypeStruct((seqs, block_len, qw), bf16),
        grid_spec=pltpu.PrefetchScalarGridSpec(
            num_scalar_prefetch=3,
            grid=(seqs,),
            in_specs=[
                seq_spec(qw),
                seq_spec(2 * kw),
                pl.BlockSpec(arrived.shape, lambda i, *_: (0, 0, 0, 0)),
            ],
            out_specs=seq_spec(qw),
            scratch_shapes=[
                pltpu.VMEM((tiles, rows, w), bf16),
                pltpu.VMEM((keep, tiles, rows, block_len), jnp.float32),
                pltpu.VMEM((tiles, rows, block_len), jnp.float32),
                pltpu.VMEM((tiles, rows, block_len), jnp.float32),
                pltpu.VMEM((tiles, rows, w), jnp.float32),
            ],
        ),
        compiler_params=pltpu.CompilerParams(vmem_limit_bytes=VMEM_LIMIT),
    )(lengths, picked, rank, queries, local, arrived)

    out_cols = w_output.shape[1]
    return pl.pallas_call(
        functools.partial(mix_kernel, tp),
        out_shape=jax.ShapeDtypeStruct((seqs, block_len, out_cols), bf16),
        in_specs=[vmem, vmem],
        out_specs=vmem,
        scratch_shapes=[
            pltpu.VMEM((tp - 1, seqs, block_len, qw), bf16),
            pltpu.VMEM((seqs, block_len, out_cols), jnp.float32),
            pltpu.SemaphoreType.DMA((tp - 1,)),
            pltpu.SemaphoreType.DMA((tp - 1,)),
        ],
        compiler_params=pltpu.CompilerParams(
            collective_id=2, has_side_effects=True, vmem_limit_bytes=VMEM_LIMIT
        ),
    )(attended, w_output)


def solution(mesh):
    return jax.shard_map(
        functools.partial(per_device, mesh.shape["kv"], mesh.shape["tp"]),
        mesh=mesh,
        in_specs=(
            P(None, "kv", None),
            P(None, "tp"),
            P(None, "tp"),
            P(None, "tp"),
            P(None, "tp"),
            P(None, "kv", None),
            P(),
        ),
        out_specs=P(None, "kv", "tp"),
        check_vma=False,
    )
```

time: 856 us -> 196 us (0.23)
  the two profiles are of different devices: /device:TPU:0 before, /device:TPU:13 now
where the time goes in v1:
time: 196 us
  Pallas kernels  190 us (97%)
  local copies, waits for them, and re-layouts  5.85 us (3%)
    pallas_call x1, Pallas kernels, per_device(): pl.pallas_call(functools.partial(exchange_kernel, n), out_shape=jax.Shape...  154 us
    pallas_call x1, Pallas kernels, per_device(): pl.pallas_call(attend_kernel, out_shape=jax.ShapeDtypeStruct((seqs, block...  15.5 us
    pallas_call x1, Pallas kernels, per_device(): pl.pallas_call(functools.partial(project_kernel, n, steps), grid=(steps,)...  10.9 us
    pallas_call x1, Pallas kernels, per_device(): pl.pallas_call(functools.partial(mix_kernel, tp), out_shape=jax.ShapeDtyp...  9.57 us

profile of v1, /device:TPU:13, one launch (start us, length us, event | category | flops | bytes accessed | tf_op | source)
XLA Modules:
  0.0 195.8 jit_solution(1796585711160664663)
XLA Ops:
  0.0 1.3 copy.9.len_ref
  1.3 10.9 %shard_map.73 = (bf16[8,128,512]{2,1,0:T(8,128)(2,1)}, bf16[8,128,512]{2,1,0:T(8,128)(2,1)}, s32[8,128]{1,0:T(8,128)}, s32[16,8,128]{2,1,0:T(8,128)}) custom-call(bf16[8,128,2048]{2,1,0:T(8,128)(2,1)} %x_ref.1, bf16[2048,512]{1,0:T(8,128)(2,1)} %wq_ref.1, bf16[2048,256]{1,0:T(8,128)(2,1)} %wk_ref.1, bf16[2048,256]{1,0:T(8,128)(2,1)} %wv_ref.1, ...), custom_call_target="tpu_custom_call" | custom-call | tf_op jit(solution)/shard_map/pallas_call | solution.py:305
  12.2 0.8 slice.3
  13.1 0.4 clamp_reduce_fusion
  13.5 0.6 reshape.3.idx_ref
  14.1 153.6 %shard_map.74.arr_ref = bf16[16,4,128,512]{3,2,1,0:T(8,128)(2,1)} custom-call(s32[64]{0:T(128)} %reshape.3.idx_ref, bf16[8,128,512]{2,1,0:T(8,128)(2,1)} %get-tuple-element.11.kv_ref), custom_call_target="tpu_custom_call" | custom-call | tf_op jit(solution)/shard_map/pallas_call | solution.py:334
  167.7 15.5 %shard_map.75.att_ref = bf16[8,128,512]{2,1,0:T(8,128)(2,1)} custom-call(s32[8]{0:T(128)} %len_ref.1, s32[8,32]{1,0:T(8,128)} %bitcast.3, s32[8,128]{1,0:T(8,128)} %get-tuple-element.9.rank_ref, bf16[8,128,512]{2,1,0:T(8,128)(2,1)} %get-tuple-element.10.q_ref, bf16[8,128,512]{2,1,0:T(8,128)(2,1)} %get-tuple-element.11.kv_ref, ...), custom_call_target="tpu_custom_call" | custom-call | tf_op jit(solution)/shard_map/pallas_call | solution.py:357
  183.2 9.6 %shard_map.76 = bf16[8,128,1024]{2,1,0:T(8,128)(2,1)} custom-call(bf16[8,128,512]{2,1,0:T(8,128)(2,1)} %shard_map.75.att_ref, bf16[1024,1024]{1,0:T(8,128)(2,1)} %w_ref.1), custom_call_target="tpu_custom_call" | custom-call | tf_op jit(solution)/shard_map/pallas_call | solution.py:381
  192.8 3.1 %copy.11 = bf16[8,128,1024]{2,1,0:T(8,128)(2,1)} copy(bf16[8,128,1024]{2,1,0:T(8,128)(2,1)} %shard_map.76) | data formatting | bytes 4194304

commit v2 on v0

v2 whole, which is shorter than its diff:
```python
import functools

import jax
import jax.numpy as jnp
from jax import lax
from jax.experimental import pallas as pl
from jax.experimental.pallas import tpu as pltpu
from jax.sharding import PartitionSpec as P

HEADS = 16
KV_HEADS = 8
HEAD_DIM = 64
LANES = 128
MESH = pl.DeviceIdType.MESH
VMEM_LIMIT = 60 * 1024 * 1024


def block_bound(rank, n):
    return n if rank == 0 else min(n, -(-7 * n // (4 * rank)))


def place(rank, head, seqs, heads):
    half = seqs // 2
    spread = max(heads // 2, 1)
    if rank < half:
        return head * half + rank, 0
    return (head % spread) * half + rank - half, 1 + head // spread


def slot_count(heads):
    spread = max(heads // 2, 1)
    return 1 + -(-heads // spread)


def ranks_of(len_ref, seqs):
    lens = [len_ref[s] for s in range(seqs)]
    ranks = []
    for s in range(seqs):
        rank = jnp.int32(0)
        for o in range(seqs):
            if o != s:
                before = lens[o] >= lens[s] if o < s else lens[o] > lens[s]
                rank = rank + before.astype(jnp.int32)
        ranks.append(rank)
    return ranks


def with_rank(ranks, k):
    found = jnp.int32(0)
    for s in range(len(ranks)):
        found = found + jnp.where(ranks[s] == k, s, 0)
    return found


def greet(axis, me, n):
    barrier = pltpu.get_barrier_semaphore()
    for k in range(1, n):
        pl.semaphore_signal(
            barrier, inc=1, device_id={axis: lax.rem(me + k, n)}, device_id_type=MESH
        )
    return barrier


def project_kernel(
    n, steps, x_ref, wq_ref, wk_ref, wv_ref, chosen_ref,
    local_ref, got_ref, incoming_ref, req_ref, send_sem, recv_sem,
):
    step = pl.program_id(0)
    me = lax.axis_index("kv")
    seqs, slots = chosen_ref.shape
    seqs_now, block_len, width = x_ref.shape

    def list_copy(dest, slot, k=0):
        return pltpu.make_async_remote_copy(
            src_ref=req_ref,
            dst_ref=incoming_ref.at[slot],
            send_sem=send_sem.at[k],
            recv_sem=recv_sem.at[slot],
            device_id={"kv": dest},
            device_id_type=MESH,
        )

    @pl.when(step == 0)
    def _():
        greet("kv", me, n)
        fill = jnp.full((seqs, LANES - slots), -1, jnp.int32)
        lists = jnp.concatenate([chosen_ref[...], fill], axis=1)
        req_ref[...] = lists
        incoming_ref[me] = lists

    rows = x_ref[...].reshape(seqs_now * block_len, width)
    scale = HEAD_DIM ** (-0.5)

    def project(w_ref):
        out = jnp.dot(rows, w_ref[...], preferred_element_type=jnp.float32).astype(jnp.bfloat16)
        return out.reshape(seqs_now, block_len, -1)

    q = project(wq_ref) * jnp.bfloat16(scale)
    k, v = project(wk_ref), project(wv_ref)
    qw = HEAD_DIM * (HEADS // KV_HEADS)
    for g in range(local_ref.shape[1]):
        at = slice(g * HEAD_DIM, (g + 1) * HEAD_DIM)
        local_ref[:, g, :, :qw] = q[:, :, g * qw : (g + 1) * qw]
        local_ref[:, g, :, qw:] = jnp.concatenate([k[:, :, at], v[:, :, at]], axis=2)

    @pl.when(step == 0)
    def _():
        pl.semaphore_wait(pltpu.get_barrier_semaphore(), n - 1)
        for j in range(1, n):
            list_copy(lax.rem(me + j, n), me, j).start()

    @pl.when(step == steps - 1)
    def _():
        for j in range(1, n):
            list_copy(lax.rem(me + j, n), me, j).wait_send()
        for j in range(1, n):
            other = lax.rem(me + j, n)
            list_copy(other, other).wait_recv()
        got_ref[...] = incoming_ref[...]


def exchange_kernel(n, len_ref, local_ref, arrived_ref, pack_ref, send_sem, recv_sem, own_sem):
    me = lax.axis_index("kv")
    seqs, heads = local_ref.shape[:2]
    barrier = greet("kv", me, n)
    ranks = ranks_of(len_ref, seqs)
    units = [(k, g) for k in range(seqs) for g in range(heads)]
    for k in range(seqs):
        s = with_rank(ranks, k)
        for g in range(heads):
            pack_ref[k, g] = local_ref[s, g]
    pl.semaphore_wait(barrier, n - 1)

    def copy(k, g, dest, slot, source):
        return pltpu.make_async_remote_copy(
            src_ref=pack_ref.at[k, g],
            dst_ref=arrived_ref.at[slot, source],
            send_sem=send_sem.at[k, g],
            recv_sem=recv_sem.at[slot, source],
            device_id={"kv": dest},
            device_id_type=MESH,
        )

    def own_copy(k, g, slot):
        return pltpu.make_async_copy(pack_ref.at[k, g], arrived_ref.at[slot, me], own_sem.at[slot])

    for k, g in units:
        owner, slot = place(k, g, seqs, heads)
        sends = me < block_bound(k, n)

        @pl.when(sends & (me != owner))
        def _():
            copy(k, g, owner, slot, me).start()

        @pl.when(sends & (me == owner))
        def _():
            own_copy(k, g, slot).start()

    for k, g in units:
        owner, slot = place(k, g, seqs, heads)
        bound = block_bound(k, n)

        @pl.when((me < bound) & (me != owner))
        def _():
            copy(k, g, owner, slot, me).wait_send()

        @pl.when((me < bound) & (me == owner))
        def _():
            own_copy(k, g, slot).wait()

        @pl.when(me == owner)
        def _():
            @pl.loop(0, bound)
            def _(b):
                @pl.when(b != me)
                def _():
                    copy(k, g, b, slot, b).wait_recv()


def attend_kernel(seqs, heads, sel, n, len_ref, pick_ref, arr_ref, out_ref):
    u = pl.program_id(0)
    me = lax.axis_index("kv")
    block_len = arr_ref.shape[2]
    half = seqs // 2
    group = HEADS // KV_HEADS
    qw = HEAD_DIM * group
    rows = group * block_len
    many = jnp.where(u == 0, heads, max(heads // 2, 1)) * half
    rank = lax.rem(me, half) + jnp.where(u == 0, 0, half)
    s = with_rank(ranks_of(len_ref, seqs), rank)
    length = jnp.where(me < many, len_ref[s], 0)
    live = (length + block_len - 1) // block_len
    unroll = 4
    key_at = lax.broadcasted_iota(jnp.int32, (group, block_len, block_len), 2)
    row_at = lax.broadcasted_iota(jnp.int32, (group, block_len, block_len), 1)
    causal = (key_at <= row_at).reshape(rows, block_len)
    zero = jnp.zeros((block_len, HEAD_DIM), jnp.bfloat16)

    @pl.loop(0, live)
    def _(b):
        base = (b * seqs + s) * sel
        count = jnp.int32(0)
        for j in range(min(sel, n)):
            count = count + (pick_ref[base + j] >= 0).astype(jnp.int32)
        q = arr_ref[0, b, :, :qw]
        qs = jnp.concatenate(
            [
                jnp.concatenate([q[:, h * HEAD_DIM : (h + 1) * HEAD_DIM], zero], axis=1)
                for h in range(group)
            ],
            axis=0,
        )

        def chunk(j0, first):
            blocks, scores = [], []
            for i in range(unroll):
                j = j0 + i
                valid = j < count
                c = jnp.where(valid, pick_ref[base + jnp.minimum(j, sel - 1)], b)
                kv = arr_ref[0, c, :, qw:]
                score = lax.dot_general(
                    qs, kv, (((1,), (1,)), ((), ())), preferred_element_type=jnp.float32
                )
                if first and i == 0:
                    score = jnp.where(causal, score, -1e30)
                else:
                    score = jnp.where(valid, score, -1e30)
                blocks.append(kv)
                scores.append(score)
            top = functools.reduce(jnp.maximum, scores)
            return blocks, scores, jnp.max(top, axis=1, keepdims=True)

        def weigh(blocks, scores, top):
            total, acc = None, None
            for kv, score in zip(blocks, scores):
                p = jnp.exp(score - top)
                got = jnp.dot(p.astype(jnp.bfloat16), kv, preferred_element_type=jnp.float32)
                total = p if total is None else total + p
                acc = got if acc is None else acc + got
            return jnp.sum(total, axis=1, keepdims=True), acc

        blocks, scores, top = chunk(jnp.int32(0), True)
        total, acc = weigh(blocks, scores, top)

        def more(i, carry):
            old, total, acc = carry
            blocks, scores, top = chunk(i * unroll, False)
            top = jnp.maximum(old, top)
            keep = jnp.exp(old - top)
            add, got = weigh(blocks, scores, top)
            return top, total * keep + add, acc * keep + got

        _, total, acc = lax.fori_loop(1, (count + unroll - 1) // unroll, more, (top, total, acc))
        done = acc / total
        parts = [
            done[h * block_len : (h + 1) * block_len, HEAD_DIM : 2 * HEAD_DIM] for h in range(group)
        ]
        done = jnp.concatenate(parts, axis=1)
        at = b * block_len + lax.broadcasted_iota(jnp.int32, done.shape, 0)
        out_ref[0, b] = jnp.where(at < length, done, 0.0).astype(out_ref.dtype)

    @pl.loop(live, n)
    def _(b):
        out_ref[0, b] = jnp.zeros(out_ref.shape[2:], out_ref.dtype)


def mix_kernel(
    n, tp, seqs, heads, len_ref, att_ref, w_ref, out_ref,
    back_ref, held_ref, send_sem, recv_sem, tp_send, tp_recv,
):
    me, my_tp = lax.axis_index("kv"), lax.axis_index("tp")
    block_len, qw = att_ref.shape[2:]
    hw = heads * qw
    pair = 2
    greet("kv", me, n)
    barrier = greet("tp", my_tp, tp)
    pl.semaphore_wait(barrier, n - 1 + tp - 1)
    units = [(k, g) for k in range(seqs) for g in range(heads)]

    def back_copy(k, g, slot, b):
        return pltpu.make_async_remote_copy(
            src_ref=att_ref.at[slot, b],
            dst_ref=back_ref.at[k, g],
            send_sem=send_sem.at[slot, b],
            recv_sem=recv_sem.at[k, g],
            device_id={"kv": b},
            device_id_type=MESH,
        )

    def tp_copy(k, dest):
        return pltpu.make_async_remote_copy(
            src_ref=back_ref,
            dst_ref=held_ref.at[k - 1],
            send_sem=tp_send.at[k - 1],
            recv_sem=tp_recv.at[k - 1],
            device_id={"tp": dest},
            device_id_type=MESH,
        )

    for k, g in units:
        owner, slot = place(k, g, seqs, heads)
        bound = block_bound(k, n)

        @pl.when(me == owner)
        def _():
            @pl.loop(0, bound)
            def _(b):
                @pl.when(b != me)
                def _():
                    back_copy(k, g, slot, b).start()

        @pl.when((me == owner) & (me < bound))
        def _():
            back_ref[k, g] = att_ref[slot, me]

        @pl.when(me >= bound)
        def _():
            back_ref[k, g] = jnp.zeros((block_len, qw), back_ref.dtype)

    ranks = ranks_of(len_ref, seqs)
    for k, g in units:
        owner, slot = place(k, g, seqs, heads)
        bound = block_bound(k, n)

        @pl.when((me < bound) & (me != owner))
        def _():
            back_copy(k, g, slot, owner).wait_recv()

    for k in range(1, tp):
        tp_copy(k, lax.rem(my_tp + k, tp)).start()

    for k, g in units:
        owner, slot = place(k, g, seqs, heads)

        @pl.when(me == owner)
        def _():
            @pl.loop(0, block_bound(k, n))
            def _(b):
                @pl.when(b != me)
                def _():
                    back_copy(k, g, slot, b).wait_send()

    def term(i, source, owner):
        rows = jnp.concatenate(
            [
                jnp.concatenate([source[ranks[i * pair + p], g] for g in range(heads)], axis=1)
                for p in range(pair)
            ],
            axis=0,
        )
        weights = w_ref[pl.ds(pl.multiple_of(owner * hw, hw), hw), :]
        return jnp.dot(rows, weights, preferred_element_type=jnp.float32)

    totals = [term(i, back_ref, my_tp) for i in range(seqs // pair)]
    for k in range(1, tp):
        tp_copy(k, lax.rem(my_tp + k, tp)).wait()
        owner = lax.rem(my_tp + tp - k, tp)
        totals = [t + term(i, held_ref.at[k - 1], owner) for i, t in enumerate(totals)]
    for i, total in enumerate(totals):
        out_ref[i * pair : (i + 1) * pair] = total.reshape(pair, block_len, -1).astype(out_ref.dtype)


def per_device(n, tp, tokens, w_query, w_key, w_value, w_output, chosen, lengths):
    seqs, block_len, width = tokens.shape
    qw, kw = w_query.shape[1], w_key.shape[1]
    heads = kw // HEAD_DIM
    group = HEADS // KV_HEADS
    unit = HEAD_DIM * (group + 2)
    slots = slot_count(heads)
    sel = chosen.shape[2]
    bf16 = jnp.bfloat16
    picked = chosen[:, 0, :]
    vmem = pl.BlockSpec(memory_space=pltpu.VMEM)
    smem = pl.BlockSpec(memory_space=pltpu.SMEM)
    steps = 4
    part = seqs // steps

    def whole(shape):
        return pl.BlockSpec(shape, lambda i: (0,) * len(shape))

    local, lists = pl.pallas_call(
        functools.partial(project_kernel, n, steps),
        grid=(steps,),
        out_shape=(
            jax.ShapeDtypeStruct((seqs, heads, block_len, unit), bf16),
            jax.ShapeDtypeStruct((n, seqs, LANES), jnp.int32),
        ),
        in_specs=[
            pl.BlockSpec((part, block_len, width), lambda i: (i, 0, 0)),
            whole((width, qw)), whole((width, kw)), whole((width, kw)), whole(picked.shape),
        ],
        out_specs=[
            pl.BlockSpec((part, heads, block_len, unit), lambda i: (i, 0, 0, 0)),
            whole((n, seqs, LANES)),
        ],
        scratch_shapes=[
            pltpu.VMEM((n, seqs, LANES), jnp.int32),
            pltpu.VMEM((seqs, LANES), jnp.int32),
            pltpu.SemaphoreType.DMA((n,)),
            pltpu.SemaphoreType.DMA((n,)),
        ],
        compiler_params=pltpu.CompilerParams(
            collective_id=0, has_side_effects=True, vmem_limit_bytes=VMEM_LIMIT
        ),
    )(tokens, w_query, w_key, w_value, picked)

    arrived = pl.pallas_call(
        functools.partial(exchange_kernel, n),
        out_shape=jax.ShapeDtypeStruct((slots, n, block_len, unit), bf16),
        in_specs=[smem, vmem],
        out_specs=pl.BlockSpec(memory_space=pl.ANY),
        scratch_shapes=[
            pltpu.VMEM((seqs, heads, block_len, unit), bf16),
            pltpu.SemaphoreType.DMA((seqs, heads)),
            pltpu.SemaphoreType.DMA((slots, n)),
            pltpu.SemaphoreType.DMA((slots,)),
        ],
        compiler_params=pltpu.CompilerParams(
            collective_id=1, has_side_effects=True, vmem_limit_bytes=VMEM_LIMIT
        ),
    )(lengths, local)

    attended = pl.pallas_call(
        functools.partial(attend_kernel, seqs, heads, sel, n),
        out_shape=jax.ShapeDtypeStruct((slots, n, block_len, HEAD_DIM * group), bf16),
        grid_spec=pltpu.PrefetchScalarGridSpec(
            num_scalar_prefetch=2,
            grid=(slots,),
            in_specs=[pl.BlockSpec((1, n, block_len, unit), lambda i, *_: (i, 0, 0, 0))],
            out_specs=pl.BlockSpec(
                (1, n, block_len, HEAD_DIM * group), lambda i, *_: (i, 0, 0, 0)
            ),
        ),
        compiler_params=pltpu.CompilerParams(vmem_limit_bytes=VMEM_LIMIT),
    )(lengths, lists[:, :, :sel].reshape(n * seqs * sel), arrived)

    out_cols = w_output.shape[1]
    back = (seqs, heads, block_len, HEAD_DIM * group)
    return pl.pallas_call(
        functools.partial(mix_kernel, n, tp, seqs, heads),
        out_shape=jax.ShapeDtypeStruct((seqs, block_len, out_cols), bf16),
        in_specs=[smem, vmem, vmem],
        out_specs=vmem,
        scratch_shapes=[
            pltpu.VMEM(back, bf16),
            pltpu.VMEM((tp - 1,) + back, bf16),
            pltpu.SemaphoreType.DMA((slots, n)),
            pltpu.SemaphoreType.DMA((seqs, heads)),
            pltpu.SemaphoreType.DMA((tp - 1,)),
            pltpu.SemaphoreType.DMA((tp - 1,)),
        ],
        compiler_params=pltpu.CompilerParams(
            collective_id=2, has_side_effects=True, vmem_limit_bytes=VMEM_LIMIT
        ),
    )(lengths, attended, w_output)


def solution(mesh):
    return jax.shard_map(
        functools.partial(per_device, mesh.shape["kv"], mesh.shape["tp"]),
        mesh=mesh,
        in_specs=(
            P(None, "kv", None),
            P(None, "tp"),
            P(None, "tp"),
            P(None, "tp"),
            P(None, "tp"),
            P(None, "kv", None),
            P(),
        ),
        out_specs=P(None, "kv", "tp"),
        check_vma=False,
    )
```

time: 856 us -> 103 us (0.12)
  local copies, waits for them, and re-layouts: 258 us -> 4.59 us
  other arithmetic: 215 us -> 0 us
  waiting for transfers between devices: 192 us -> 0 us
  matrix products: 158 us -> 0 us
  Pallas kernels: 0 us -> 97.6 us
  starting transfers between devices: 15.2 us -> 0 us
  between operations: 13.5 us -> 0.03 us
    sub x10 -> x0, other arithmetic: 167 us -> none  [the longest x8 167 us: attend(): exponent = jnp.exp(masked - row_max)]
    dot_general x20 -> x0, matrix products: 158 us -> none  [the longest x8 77.5 us: attend(): jnp.einsum('qkgd,nkd->kgqn', grouped, key_rows, preferred_element_type=jn...]
    all_to_all x2 -> x0, waiting for transfers between devices: 148 us -> none  [the longest x1 148 us: per_device(): lax.all_to_all(outgoing, 'kv', split_axis=0, concat_axis=0, tiled=True)]
    slice x24 -> x0, local copies, waits for them, and re-layouts: 111 us -> none  [the longest x16 74.6 us: attend(): fetched[:, :, key_width:]]
    pallas_call x0 -> x4, Pallas kernels: none -> 97.6 us  [the longest x1 33 us: per_device(): pl.pallas_call(functools.partial(exchange_kernel, n), out_shape=jax.Shape...]
    reshape x17 -> x1, local copies, waits for them, and re-layouts: 68.1 us -> 1.51 us  [per_device(): lists[:, :, :sel].reshape(n * seqs * sel)]
    gather x12 -> x0, local copies, waits for them, and re-layouts: 58.4 us -> none  [the longest x8 51.4 us: attend(): fetched = key_lookup[source_row]]
    all_gather x1 -> x0, waiting for transfers between devices: 44.5 us -> none  [per_device(): lax.all_gather(attended_rows, 'tp', axis=1, tiled=True)]
  transfers between devices with their start and end apart: 3 -> 0, of which waited for: 2 -> 0; matrix products, arithmetic and copies ran while one was open for 2% -> 0% of each run, Pallas kernels for 0% -> 0%
where the time goes in v2:
time: 103 us; the launch traced here: 102 us
  Pallas kernels  97.6 us (95%)
  local copies, waits for them, and re-layouts  4.59 us (4%)
    pallas_call x1, Pallas kernels, per_device(): pl.pallas_call(functools.partial(exchange_kernel, n), out_shape=jax.Shape...  33 us
    pallas_call x1, Pallas kernels, per_device(): pl.pallas_call(functools.partial(attend_kernel, seqs, heads, sel, n), out...  25.8 us
    pallas_call x1, Pallas kernels, per_device(): pl.pallas_call(functools.partial(mix_kernel, n, tp, seqs, heads), out_sha...  24.1 us
    pallas_call x1, Pallas kernels, per_device(): pl.pallas_call(functools.partial(project_kernel, n, steps), grid=(steps,)...  14.8 us
    unnamed x1, local copies, waits for them, and re-layouts  3.08 us

profile of v2, /device:TPU:0, one launch (start us, length us, event | category | flops | bytes accessed | tf_op | source)
XLA Modules:
  0.0 102.2 jit_solution(6431104599943525816)
XLA Ops:
  0.0 14.8 %shard_map.73 = (bf16[8,4,128,256]{3,2,1,0:T(8,128)(2,1)}, s32[16,8,128]{2,1,0:T(8,128)}) custom-call(bf16[8,128,2048]{2,1,0:T(8,128)(2,1)} %x_ref.1, bf16[2048,512]{1,0:T(8,128)(2,1)} %wq_ref.1, bf16[2048,256]{1,0:T(8,128)(2,1)} %wk_ref.1, bf16[2048,256]{1,0:T(8,128)(2,1)} %wv_ref.1, s32[8,32]{1,0:T(8,128)} %bitcast.3), custom_call_target="tpu_custom_call" | custom-call | tf_op jit(solution)/shard_map/pallas_call | solution.py:381
  14.8 1.5 %reshape.3.pick_ref = s32[4096]{0:T(1024)} reshape(s32[16,8,32]{2,1,0:T(8,128)} %bitcast.2) | data formatting | bytes 32768 | tf_op jit(solution)/shard_map/reshape | solution.py:435
  16.3 33.0 %shard_map.74.arr_ref = bf16[3,16,128,256]{3,2,1,0:T(8,128)(2,1)} custom-call(s32[8]{0:T(128)} %len_ref.5, bf16[8,4,128,256]{3,2,1,0:T(8,128)(2,1)} %get-tuple-element.8.local_ref), custom_call_target="tpu_custom_call" | custom-call | tf_op jit(solution)/shard_map/pallas_call | solution.py:407
  49.3 25.8 %shard_map.75.att_ref = bf16[3,16,128,128]{3,2,1,0:T(8,128)(2,1)} custom-call(s32[8]{0:T(128)} %len_ref.5, s32[4096]{0:T(1024)} %reshape.3.pick_ref, bf16[3,16,128,256]{3,2,1,0:T(8,128)(2,1)} %shard_map.74.arr_ref), custom_call_target="tpu_custom_call" | custom-call | tf_op jit(solution)/shard_map/pallas_call | solution.py:423
  75.0 24.1 %shard_map.76 = bf16[8,128,1024]{2,1,0:T(8,128)(2,1)} custom-call(s32[8]{0:T(128)} %len_ref.5, bf16[3,16,128,128]{3,2,1,0:T(8,128)(2,1)} %shard_map.75.att_ref, bf16[1024,1024]{1,0:T(8,128)(2,1)} %w_ref.1), custom_call_target="tpu_custom_call" | custom-call | tf_op jit(solution)/shard_map/pallas_call | solution.py:439
  99.2 3.1 %copy.9 = bf16[8,128,1024]{2,1,0:T(8,128)(2,1)} copy(bf16[8,128,1024]{2,1,0:T(8,128)(2,1)} %shard_map.76) | data formatting | bytes 4194304

commit v3 on v2

--- a/solution.py
+++ b/solution.py
@@ -61,75 +61,34 @@
     return barrier
 
 
-def project_kernel(
-    n, steps, x_ref, wq_ref, wk_ref, wv_ref, chosen_ref,
-    local_ref, got_ref, incoming_ref, req_ref, send_sem, recv_sem,
+def project_send_kernel(
+    n, x_ref, wq_ref, wk_ref, wv_ref, chosen_ref, len_ref, got_ref, arrived_ref,
+    incoming_ref, req_ref, pack_ref, list_send, list_recv, send_sem, recv_sem, own_sem,
 ):
-    step = pl.program_id(0)
     me = lax.axis_index("kv")
     seqs, slots = chosen_ref.shape
-    seqs_now, block_len, width = x_ref.shape
+    heads = pack_ref.shape[1]
+    block_len = x_ref.shape[1]
+    barrier = greet("kv", me, n)
+    ranks = ranks_of(len_ref, seqs)
+    units = [(k, g) for k in range(seqs) for g in range(heads)]
+    pair = 2
+    scale = HEAD_DIM ** (-0.5)
+    qw = HEAD_DIM * (HEADS // KV_HEADS)
+    fill = jnp.full((seqs, LANES - slots), -1, jnp.int32)
+    lists = jnp.concatenate([chosen_ref[...], fill], axis=1)
+    req_ref[...] = lists
+    incoming_ref[me] = lists
 
     def list_copy(dest, slot, k=0):
         return pltpu.make_async_remote_copy(
             src_ref=req_ref,
             dst_ref=incoming_ref.at[slot],
-            send_sem=send_sem.at[k],
-            recv_sem=recv_sem.at[slot],
+            send_sem=list_send.at[k],
+            recv_sem=list_recv.at[slot],
             device_id={"kv": dest},
             device_id_type=MESH,
         )
-
-    @pl.when(step == 0)
-    def _():
-        greet("kv", me, n)
-        fill = jnp.full((seqs, LANES - slots), -1, jnp.int32)
-        lists = jnp.concatenate([chosen_ref[...], fill], axis=1)
-        req_ref[...] = lists
-        incoming_ref[me] = lists
-
-    rows = x_ref[...].reshape(seqs_now * block_len, width)
-    scale = HEAD_DIM ** (-0.5)
-
-    def project(w_ref):
-        out = jnp.dot(rows, w_ref[...], preferred_element_type=jnp.float32).astype(jnp.bfloat16)
-        return out.reshape(seqs_now, block_len, -1)
-
-    q = project(wq_ref) * jnp.bfloat16(scale)
-    k, v = project(wk_ref), project(wv_ref)
-    qw = HEAD_DIM * (HEADS // KV_HEADS)
-    for g in range(local_ref.shape[1]):
-        at = slice(g * HEAD_DIM, (g + 1) * HEAD_DIM)
-        local_ref[:, g, :, :qw] = q[:, :, g * qw : (g + 1) * qw]
-        local_ref[:, g, :, qw:] = jnp.concatenate([k[:, :, at], v[:, :, at]], axis=2)
-
-    @pl.when(step == 0)
-    def _():
-        pl.semaphore_wait(pltpu.get_barrier_semaphore(), n - 1)
-        for j in range(1, n):
-            list_copy(lax.rem(me + j, n), me, j).start()
-
-    @pl.when(step == steps - 1)
-    def _():
-        for j in range(1, n):
-            list_copy(lax.rem(me + j, n), me, j).wait_send()
-        for j in range(1, n):
-            other = lax.rem(me + j, n)
-            list_copy(other, other).wait_recv()
-        got_ref[...] = incoming_ref[...]
-
-
-def exchange_kernel(n, len_ref, local_ref, arrived_ref, pack_ref, send_sem, recv_sem, own_sem):
-    me = lax.axis_index("kv")
-    seqs, heads = local_ref.shape[:2]
-    barrier = greet("kv", me, n)
-    ranks = ranks_of(len_ref, seqs)
-    units = [(k, g) for k in range(seqs) for g in range(heads)]
-    for k in range(seqs):
-        s = with_rank(ranks, k)
-        for g in range(heads):
-            pack_ref[k, g] = local_ref[s, g]
-    pl.semaphore_wait(barrier, n - 1)
 
     def copy(k, g, dest, slot, source):
         return pltpu.make_async_remote_copy(
@@ -144,17 +103,48 @@
     def own_copy(k, g, slot):
         return pltpu.make_async_copy(pack_ref.at[k, g], arrived_ref.at[slot, me], own_sem.at[slot])
 
-    for k, g in units:
-        owner, slot = place(k, g, seqs, heads)
-        sends = me < block_bound(k, n)
-
-        @pl.when(sends & (me != owner))
-        def _():
-            copy(k, g, owner, slot, me).start()
-
-        @pl.when(sends & (me == owner))
-        def _():
-            own_copy(k, g, slot).start()
+    for first in range(0, seqs, pair):
+        rows = jnp.concatenate(
+            [x_ref[with_rank(ranks, first + p)] for p in range(pair)], axis=0
+        )
+
+        def project(w_ref):
+            out = jnp.dot(rows, w_ref[...], preferred_element_type=jnp.float32)
+            return out.astype(jnp.bfloat16).reshape(pair, block_len, -1)
+
+        q = project(wq_ref) * jnp.bfloat16(scale)
+        keys, values = project(wk_ref), project(wv_ref)
+        for p in range(pair):
+            for g in range(heads):
+                at = slice(g * HEAD_DIM, (g + 1) * HEAD_DIM)
+                pack_ref[first + p, g, :, :qw] = q[p, :, g * qw : (g + 1) * qw]
+                pack_ref[first + p, g, :, qw:] = jnp.concatenate(
+                    [keys[p, :, at], values[p, :, at]], axis=1
+                )
+        if first == 0:
+            pl.semaphore_wait(barrier, n - 1)
+        for k, g in units[first * heads : (first + pair) * heads]:
+            owner, slot = place(k, g, seqs, heads)
+            sends = me < block_bound(k, n)
+
+            @pl.when(sends & (me != owner))
+            def _():
+                copy(k, g, owner, slot, me).start()
+
+            @pl.when(sends & (me == owner))
+            def _():
+                own_copy(k, g, slot).start()
+
+        if first == 0:
+            for j in range(1, n):
+                list_copy(lax.rem(me + j, n), me, j).start()
+
+    for j in range(1, n):
+        list_copy(lax.rem(me + j, n), me, j).wait_send()
+    for j in range(1, n):
+        other = lax.rem(me + j, n)
+        list_copy(other, other).wait_recv()
+    got_ref[...] = incoming_ref[...]
 
     for k, g in units:
         owner, slot = place(k, g, seqs, heads)
@@ -196,8 +186,36 @@
     causal = (key_at <= row_at).reshape(rows, block_len)
     zero = jnp.zeros((block_len, HEAD_DIM), jnp.bfloat16)
 
-    @pl.loop(0, live)
-    def _(b):
+    def chunk(row, j0, first):
+        b, base, count, qs = row
+        blocks, scores = [], []
+        for i in range(unroll):
+            j = j0 + i
+            valid = j < count
+            c = jnp.where(valid, pick_ref[base + jnp.minimum(j, sel - 1)], b)
+            kv = arr_ref[0, c, :, qw:]
+            score = lax.dot_general(
+                qs, kv, (((1,), (1,)), ((), ())), preferred_element_type=jnp.float32
+            )
+            if first and i == 0:
+                score = jnp.where(causal, score, -1e30)
+            else:
+                score = jnp.where(valid, score, -1e30)
+            blocks.append(kv)
+            scores.append(score)
+        top = functools.reduce(jnp.maximum, scores)
+        return blocks, scores, jnp.max(top, axis=1, keepdims=True)
+
+    def weigh(blocks, scores, top):
+        total, acc = None, None
+        for kv, score in zip(blocks, scores):
+            p = jnp.exp(score - top)
+            got = jnp.dot(p.astype(jnp.bfloat16), kv, preferred_element_type=jnp.float32)
+            total = p if total is None else total + p
+            acc = got if acc is None else acc + got
+        return jnp.sum(total, axis=1, keepdims=True), acc
+
+    def row_of(b):
         base = (b * seqs + s) * sel
         count = jnp.int32(0)
         for j in range(min(sel, n)):
@@ -210,54 +228,38 @@
             ],
             axis=0,
         )
-
-        def chunk(j0, first):
-            blocks, scores = [], []
-            for i in range(unroll):
-                j = j0 + i
-                valid = j < count
-                c = jnp.where(valid, pick_ref[base + jnp.minimum(j, sel - 1)], b)
-                kv = arr_ref[0, c, :, qw:]
-                score = lax.dot_general(
-                    qs, kv, (((1,), (1,)), ((), ())), preferred_element_type=jnp.float32
-                )
-                if first and i == 0:
-                    score = jnp.where(causal, score, -1e30)
-                else:
-                    score = jnp.where(valid, score, -1e30)
-                blocks.append(kv)
-                scores.append(score)
-            top = functools.reduce(jnp.maximum, scores)
-            return blocks, scores, jnp.max(top, axis=1, keepdims=True)
-
-        def weigh(blocks, scores, top):
-            total, acc = None, None
-            for kv, score in zip(blocks, scores):
-                p = jnp.exp(score - top)
-                got = jnp.dot(p.astype(jnp.bfloat16), kv, preferred_element_type=jnp.float32)
-                total = p if total is None else total + p
-                acc = got if acc is None else acc + got
-            return jnp.sum(total, axis=1, keepdims=True), acc
-
-        blocks, scores, top = chunk(jnp.int32(0), True)
-        total, acc = weigh(blocks, scores, top)
-
-        def more(i, carry):
-            old, total, acc = carry
-            blocks, scores, top = chunk(i * unroll, False)
-            top = jnp.maximum(old, top)
-            keep = jnp.exp(old - top)
-            add, got = weigh(blocks, scores, top)
-            return top, total * keep + add, acc * keep + got
-
-        _, total, acc = lax.fori_loop(1, (count + unroll - 1) // unroll, more, (top, total, acc))
-        done = acc / total
-        parts = [
-            done[h * block_len : (h + 1) * block_len, HEAD_DIM : 2 * HEAD_DIM] for h in range(group)
-        ]
-        done = jnp.concatenate(parts, axis=1)
-        at = b * block_len + lax.broadcasted_iota(jnp.int32, done.shape, 0)
-        out_ref[0, b] = jnp.where(at < length, done, 0.0).astype(out_ref.dtype)
+        return b, base, count, qs
+
+    @pl.loop(0, (live + 1) // 2)
+    def _(i):
+        both = [row_of(i), row_of(live - 1 - i)]
+        opened = [chunk(row, jnp.int32(0), True) for row in both]
+        begun = []
+        for blocks, scores, top in opened:
+            total, acc = weigh(blocks, scores, top)
+            begun.append((top, total, acc))
+
+        def more(at, carry):
+            opened = [chunk(row, at * unroll, False) for row in both]
+            kept = []
+            for (old, total, acc), (blocks, scores, top) in zip(carry, opened):
+                top = jnp.maximum(old, top)
+                keep = jnp.exp(old - top)
+                add, got = weigh(blocks, scores, top)
+                kept.append((top, total * keep + add, acc * keep + got))
+            return tuple(kept)
+
+        longest = jnp.maximum(both[0][2], both[1][2])
+        ended = lax.fori_loop(1, (longest + unroll - 1) // unroll, more, tuple(begun))
+        for (b, _, _, _), (_, total, acc) in zip(both, ended):
+            done = acc / total
+            parts = [
+                done[h * block_len : (h + 1) * block_len, HEAD_DIM : 2 * HEAD_DIM]
+                for h in range(group)
+            ]
+            done = jnp.concatenate(parts, axis=1)
+            at = b * block_len + lax.broadcasted_iota(jnp.int32, done.shape, 0)
+            out_ref[0, b] = jnp.where(at < length, done, 0.0).astype(out_ref.dtype)
 
     @pl.loop(live, n)
     def _(b):
@@ -372,53 +374,28 @@
     picked = chosen[:, 0, :]
     vmem = pl.BlockSpec(memory_space=pltpu.VMEM)
     smem = pl.BlockSpec(memory_space=pltpu.SMEM)
-    steps = 4
-    part = seqs // steps
-
-    def whole(shape):
-        return pl.BlockSpec(shape, lambda i: (0,) * len(shape))
-
-    local, lists = pl.pallas_call(
-        functools.partial(project_kernel, n, steps),
-        grid=(steps,),
+    lists, arrived = pl.pallas_call(
+        functools.partial(project_send_kernel, n),
         out_shape=(
-            jax.ShapeDtypeStruct((seqs, heads, block_len, unit), bf16),
             jax.ShapeDtypeStruct((n, seqs, LANES), jnp.int32),
+            jax.ShapeDtypeStruct((slots, n, block_len, unit), bf16),
         ),
-        in_specs=[
-            pl.BlockSpec((part, block_len, width), lambda i: (i, 0, 0)),
-            whole((width, qw)), whole((width, kw)), whole((width, kw)), whole(picked.shape),
-        ],
-        out_specs=[
-            pl.BlockSpec((part, heads, block_len, unit), lambda i: (i, 0, 0, 0)),
-            whole((n, seqs, LANES)),
-        ],
+        in_specs=[vmem, vmem, vmem, vmem, vmem, smem],
+        out_specs=[vmem, pl.BlockSpec(memory_space=pl.ANY)],
         scratch_shapes=[
             pltpu.VMEM((n, seqs, LANES), jnp.int32),
             pltpu.VMEM((seqs, LANES), jnp.int32),
+            pltpu.VMEM((seqs, heads, block_len, unit), bf16),
             pltpu.SemaphoreType.DMA((n,)),
             pltpu.SemaphoreType.DMA((n,)),
-        ],
-        compiler_params=pltpu.CompilerParams(
-            collective_id=0, has_side_effects=True, vmem_limit_bytes=VMEM_LIMIT
-        ),
-    )(tokens, w_query, w_key, w_value, picked)
-
-    arrived = pl.pallas_call(
-        functools.partial(exchange_kernel, n),
-        out_shape=jax.ShapeDtypeStruct((slots, n, block_len, unit), bf16),
-        in_specs=[smem, vmem],
-        out_specs=pl.BlockSpec(memory_space=pl.ANY),
-        scratch_shapes=[
-            pltpu.VMEM((seqs, heads, block_len, unit), bf16),
             pltpu.SemaphoreType.DMA((seqs, heads)),
             pltpu.SemaphoreType.DMA((slots, n)),
             pltpu.SemaphoreType.DMA((slots,)),
         ],
         compiler_params=pltpu.CompilerParams(
-            collective_id=1, has_side_effects=True, vmem_limit_bytes=VMEM_LIMIT
+            collective_id=0, has_side_effects=True, vmem_limit_bytes=VMEM_LIMIT
         ),
-    )(lengths, local)
+    )(tokens, w_query, w_key, w_value, picked, lengths)
 
     attended = pl.pallas_call(
         functools.partial(attend_kernel, seqs, heads, sel, n),

time: 103 us -> 93.2 us (0.905)
  Pallas kernels: 97.6 us -> 88.3 us
    pallas_call x2 -> x1, Pallas kernels: 47.7 us -> 41.4 us  [per_device(): pl.pallas_call(functools.partial(project_send_kernel, n), out_shape=(jax....]
    pallas_call x1, Pallas kernels: 25.8 us -> 21.7 us  [per_device(): pl.pallas_call(functools.partial(attend_kernel, seqs, heads, sel, n), out...]
    pallas_call x1, Pallas kernels: 24.1 us -> 25.2 us  [per_device(): pl.pallas_call(functools.partial(mix_kernel, n, tp, seqs, heads), out_sha...]
where the time goes in v3:
time: 93.2 us; the launch traced here: 92.9 us
  Pallas kernels  88.3 us (95%)
  local copies, waits for them, and re-layouts  4.6 us (5%)
    pallas_call x1, Pallas kernels, per_device(): pl.pallas_call(functools.partial(project_send_kernel, n), out_shape=(jax....  41.4 us
    pallas_call x1, Pallas kernels, per_device(): pl.pallas_call(functools.partial(mix_kernel, n, tp, seqs, heads), out_sha...  25.2 us
    pallas_call x1, Pallas kernels, per_device(): pl.pallas_call(functools.partial(attend_kernel, seqs, heads, sel, n), out...  21.7 us
    unnamed x1, local copies, waits for them, and re-layouts  3.08 us

profile of v3, /device:TPU:0, one launch (start us, length us, event | category | flops | bytes accessed | tf_op | source)
XLA Modules:
  0.0 92.9 jit_solution(675740852884326280)
XLA Ops:
  0.0 41.4 %shard_map.73 = (s32[16,8,128]{2,1,0:T(8,128)}, bf16[3,16,128,256]{3,2,1,0:T(8,128)(2,1)}) custom-call(bf16[8,128,2048]{2,1,0:T(8,128)(2,1)} %x_ref.1, bf16[2048,512]{1,0:T(8,128)(2,1)} %wq_ref.1, bf16[2048,256]{1,0:T(8,128)(2,1)} %wk_ref.1, bf16[2048,256]{1,0:T(8,128)(2,1)} %wv_ref.1, s32[8,32]{1,0:T(8,128)} %bitcast.3, s32[8]{0:T(128)} %len_ref.5), custom_call_target="tpu_custom_call" | custom-call | tf_op jit(solution)/shard_map/pallas_call | solution.py:377
  41.4 1.5 %reshape.3.pick_ref = s32[4096]{0:T(1024)} reshape(s32[16,8,32]{2,1,0:T(8,128)} %bitcast.2) | data formatting | bytes 32768 | tf_op jit(solution)/shard_map/reshape | solution.py:412
  42.9 21.7 %shard_map.74.att_ref = bf16[3,16,128,128]{3,2,1,0:T(8,128)(2,1)} custom-call(s32[8]{0:T(128)} %len_ref.5, s32[4096]{0:T(1024)} %reshape.3.pick_ref, bf16[3,16,128,256]{3,2,1,0:T(8,128)(2,1)} %get-tuple-element.8.arr_ref), custom_call_target="tpu_custom_call" | custom-call | tf_op jit(solution)/shard_map/pallas_call | solution.py:400
  64.7 25.2 %shard_map.75 = bf16[8,128,1024]{2,1,0:T(8,128)(2,1)} custom-call(s32[8]{0:T(128)} %len_ref.5, bf16[3,16,128,128]{3,2,1,0:T(8,128)(2,1)} %shard_map.74.att_ref, bf16[1024,1024]{1,0:T(8,128)(2,1)} %w_ref.1), custom_call_target="tpu_custom_call" | custom-call | tf_op jit(solution)/shard_map/pallas_call | solution.py:416
  89.8 3.1 %copy.9 = bf16[8,128,1024]{2,1,0:T(8,128)(2,1)} copy(bf16[8,128,1024]{2,1,0:T(8,128)(2,1)} %shard_map.75) | data formatting | bytes 4194304
